TPU v7x, 32 devices: a whole 2x2x4 slice. The times are simulated.
32 devices in a mesh: ep: 4 (over y, x), tp: 8 (over z, core).
Axes of the slice: x: 2, y: 2, z: 4, core: 2. Of those that a mesh axis runs over, the one named last changes fastest.
Arguments:
- mix_tokens: bfloat16 [4096, 2048], P(('ep', 'tp')), may hold values from -6 to 6
- mix_gain: bfloat16 [2048], replicated, may hold values from 0.099609375 to 1.8984375
- gate_proj: bfloat16 [2048, 1024], P(None, 'tp'), may hold values from -0.125 to 0.125
- conv_proj: bfloat16 [2048, 1024], P(None, 'tp'), may hold values from -0.125 to 0.125
- value_proj: bfloat16 [2048, 1024], P(None, 'tp'), may hold values from -0.125 to 0.125
- conv_taps: bfloat16 [3, 1024], P(None, 'tp'), may hold values from -3 to 3
- out_proj: bfloat16 [1024, 2048], P('tp'), may hold values from -0.1875 to 0.1875
- moe_tokens: bfloat16 [2048, 2048], P(('ep', 'tp')), may hold values from -6 to 6
- moe_gain: bfloat16 [2048], replicated, may hold values from 0.099609375 to 1.8984375
- expert_ids: int32 [2048, 2], P(('ep', 'tp')), may hold values from 0 to 3, all different within a row; in each aligned block of 64 rows (0 to 63, 64 to 127, ...) at most 36 rows name the same one
- expert_scores: float32 [2048, 2], P(('ep', 'tp')), may hold values from -6 to 6
- expert_gate: bfloat16 [4, 2048, 4096], P('ep', None, 'tp'), may hold values from -0.125 to 0.125
- expert_up: bfloat16 [4, 2048, 4096], P('ep', None, 'tp'), may hold values from -0.125 to 0.125
- expert_down: bfloat16 [4, 4096, 2048], P('ep', 'tp'), may hold values from -0.09375 to 0.09375
Outputs:
- mix_out: bfloat16 [4096, 2048], P(('ep', 'tp'))
- moe_out: bfloat16 [2048, 2048], P(('ep', 'tp'))
Inputs may be any that keep to these rules, and one draw needn't show every extreme that they name: `expert_ids`: each row names 2 different experts; among the rows of one device no expert is named more than 36 times.
All inputs are finite; a program needn't handle non-finite values.
Results may differ from a plain program's by a relative error of at most 0.018.
Values may be sent and summed in bfloat16 or wider, within the bound.
A program may use at most 128 MiB of HBM per device.

v0:
```python
import jax
import jax.numpy as jnp
from jax import lax
from jax.sharding import PartitionSpec as P

norm_eps = 1e-06


def from_behind(value, axis, steps):
    count = lax.axis_size(axis)
    leading, last = (max(0, -steps), min(count, count - steps))
    return lax.ppermute(value, axis, [(source, source + steps) for source in range(leading, last)])


def scaled_norm(row_data, gain_vec):
    values = row_data.astype(jnp.float32)
    inverse = lax.rsqrt(jnp.mean(values * values, axis=1, keepdims=True) + norm_eps)
    return (values * inverse * gain_vec.astype(jnp.float32)).astype(jnp.bfloat16)


def shards(
    mix_tokens,
    mix_gain,
    gate_proj,
    conv_proj,
    value_proj,
    conv_taps,
    out_proj,
    moe_tokens,
    moe_gain,
    expert_ids,
    expert_scores,
    expert_gate,
    expert_up,
    expert_down,
):
    normed = scaled_norm(mix_tokens, mix_gain)
    w_joint = jnp.concatenate([gate_proj, conv_proj, value_proj], axis=1)
    combined = jnp.dot(
        lax.all_gather(normed, "tp", axis=0, tiled=True),
        w_joint,
        preferred_element_type=jnp.float32,
    ).astype(jnp.bfloat16)
    channels = gate_proj.shape[1]
    out_gate = combined[:, :channels]
    in_gate = combined[:, channels : 2 * channels]
    values = combined[:, 2 * channels :]
    signal = (in_gate.astype(jnp.float32) * values.astype(jnp.float32)).astype(jnp.bfloat16)
    tap_count = conv_taps.shape[0]
    before = from_behind(signal[signal.shape[0] - (tap_count - 1) :], "ep", 1)
    extended = jnp.concatenate([before, signal], axis=0)
    length = signal.shape[0]
    tap_values = conv_taps.astype(jnp.float32)
    convolved = jnp.zeros((length, channels), jnp.float32)
    for offset in range(tap_count):
        convolved = (
            convolved + extended[offset : offset + length].astype(jnp.float32) * tap_values[offset]
        )
    carried = (out_gate.astype(jnp.float32) * convolved).astype(jnp.bfloat16)
    row_block = carried
    mix_out = lax.psum_scatter(
        jnp.dot(row_block, out_proj, preferred_element_type=jnp.float32).astype(jnp.bfloat16),
        "tp",
        scatter_dimension=0,
        tiled=True,
    )
    moe_normed = scaled_norm(moe_tokens, moe_gain)
    experts = expert_gate.shape[0] * lax.axis_size("ep")
    row_count, top_count = expert_ids.shape
    capacity = top_count * row_count // experts + max(1, top_count * row_count // (8 * experts))
    width_model = moe_tokens.shape[1]
    flat_ids = expert_ids.reshape(-1)
    onehot = (flat_ids[:, None] == jnp.arange(experts, dtype=jnp.int32)[None, :]).astype(jnp.int32)
    slot_rank = jnp.sum((jnp.cumsum(onehot, axis=0) - onehot) * onehot, axis=1)
    slot_index = flat_ids * capacity + slot_rank
    slot_match = slot_index[:, None] == jnp.arange(experts * capacity, dtype=jnp.int32)[None, :]
    dispatch_map = jnp.any(
        slot_match.reshape(row_count, top_count, experts * capacity), axis=1
    ).astype(jnp.bfloat16)
    outgoing = lax.dot_general(
        dispatch_map, moe_normed, (((0,), (0,)), ((), ())), preferred_element_type=jnp.float32
    ).astype(jnp.bfloat16)
    arrived = lax.all_to_all(
        outgoing.reshape(experts, capacity, width_model),
        "ep",
        split_axis=0,
        concat_axis=0,
        tiled=True,
    )
    arrived_rows = arrived.reshape(-1, width_model)
    w_gate = expert_gate[0]
    w_up = expert_up[0]
    w_down = expert_down[0]
    portion = lax.all_gather(arrived_rows, "tp", axis=0, tiled=True)
    gate_value = jnp.dot(portion, w_gate, preferred_element_type=jnp.float32)
    up_value = jnp.dot(portion, w_up, preferred_element_type=jnp.float32)
    hidden = (jax.nn.silu(gate_value) * up_value).astype(jnp.bfloat16)
    row_block = hidden
    summed = lax.psum_scatter(
        jnp.dot(row_block, w_down, preferred_element_type=jnp.float32).astype(jnp.bfloat16),
        "tp",
        scatter_dimension=0,
        tiled=True,
    )
    returned = lax.all_to_all(
        summed.reshape(experts, capacity, width_model),
        "ep",
        split_axis=0,
        concat_axis=0,
        tiled=True,
    )
    flat_back = returned.reshape(experts * capacity, width_model)
    picked = flat_back[slot_index].reshape(row_count, top_count, width_model)
    route_weight = jax.nn.softmax(expert_scores, axis=1)
    moe_out = jnp.sum(route_weight[:, :, None] * picked.astype(jnp.float32), axis=1).astype(
        jnp.bfloat16
    )
    return (mix_out, moe_out)


def solution(mesh):
    in_specs = (
        P(("ep", "tp"), None),
        P(),
        P(None, "tp"),
        P(None, "tp"),
        P(None, "tp"),
        P(None, "tp"),
        P("tp", None),
        P(("ep", "tp"), None),
        P(),
        P(("ep", "tp"), None),
        P(("ep", "tp"), None),
        P("ep", None, "tp"),
        P("ep", None, "tp"),
        P("ep", "tp", None),
    )
    out_specs = (P(("ep", "tp"), None), P(("ep", "tp"), None))
    return jax.shard_map(shards, mesh=mesh, in_specs=in_specs, out_specs=out_specs, check_vma=False)
```

profile of v0, /device:TPU:0, one launch (start us, length us, event | category | flops | bytes accessed | tf_op | source)
XLA Modules:
  0.0 240.8 jit_solution(1236519495973544300)
XLA Ops:
  7.2 0.0 copy-start
  7.2 0.0 all-gather.5.cloned.1.call-start
  7.2 0.9 copy.23
  8.1 0.1 eq.29
  8.3 0.1 fusion.32
  8.4 0.2 reduce_window_sum.11
  8.5 0.2 select_reduce_fusion
  8.7 0.1 reduce_sum.52
  8.9 0.1 copy.25
  9.0 0.1 fusion.31
  9.1 0.7 convert_element_type.89
  9.8 1.1 fusion.19
  10.9 1.3 convolution_convert_fusion.2
  12.2 0.0 copy-start.4
  12.2 0.1 reshape.84
  12.4 14.9 %all_to_all.10 = bf16[4,36,2048]{2,1,0:T(8,128)(2,1)S(1)} all-to-all(bf16[4,36,2048]{2,1,0:T(8,128)(2,1)S(1)} %reshape.84), channel_id=1, replica_groups=mesh['ep'=4,'tp'=8] {'ep'}, dimensions={0} | all-to-all | bytes 1179648 | tf_op jit(solution)/shard_map/all_to_all | solution.py:83
  27.3 0.9 reshape.85
  28.2 0.0 all-gather.5.cloned.1.call-update
  28.2 0.0 all-gather.3.cloned.1.call-start
  28.3 1.2 fusion.14
  29.5 1.0 fusion.16
  30.5 0.0 all-gather.3.cloned.1.call-update
  30.5 0.0 reduce-scatter.5.cloned.1.call-start
  30.6 48.7 %all-gather.5.cloned.1.call-done = bf16[1152,2048]{1,0:T(8,128)(2,1)} async-done(((bf16[144,2048]{1,0:T(8,128)(2,1)}), bf16[1152,2048]{1,0:T(8,128)(2,1)}) %all-gather.5.cloned.1.call-update) | async-done | bytes 4718608 | tf_op jit(solution)/shard_map/all_gather | solution.py:94
  79.3 7.0 %fusion.3 = f32[1152,512]{1,0:T(8,128)} fusion(bf16[1152,2048]{1,0:T(8,128)(2,1)} %all-gather.5.cloned.1.call-done, bf16[1,2048,512]{2,1,0:T(8,128)(2,1)} %param.25), kind=kOutput, calls=%fused_computation.8 | convolution fusion | flops 2415919104 | bytes 9175040 | tf_op jit(solution)/shard_map/dot_general | solution.py:95
  86.3 11.6 %convolution_convert_fusion = bf16[1152,2048]{1,0:T(8,128)(2,1)} fusion(bf16[1,512,2048]{2,1,0:T(8,128)(2,1)S(1)} %copy-done, bf16[1152,2048]{1,0:T(8,128)(2,1)} %all-gather.5.cloned.1.call-done, f32[1152,512]{1,0:T(8,128)} %fusion.3, bf16[1,2048,512]{2,1,0:T(8,128)(2,1)} %param.26), kind=kOutput, calls=%fused_computation.1 | convolution fusion | flops 4837736448 | bytes 15990784 | tf_op jit(solution)/shard_map/dot_general | solution.py:100
  97.9 0.0 reduce-scatter.5.cloned.1.call-update
  98.0 0.0 reduce-scatter.3.cloned.1.call-start
  98.0 0.6 copy-done.5
  98.6 28.5 %all-gather.3.cloned.1.call-done = bf16[1024,2048]{1,0:T(8,128)(2,1)} async-done(((bf16[128,2048]{1,0:T(8,128)(2,1)}), bf16[1024,2048]{1,0:T(8,128)(2,1)}) %all-gather.3.cloned.1.call-update) | async-done | bytes 4194320 | tf_op jit(solution)/shard_map/all_gather | solution.py:40
  127.1 4.8 %fusion.11 = bf16[1024,384]{1,0:T(8,128)(2,1)S(1)} fusion(bf16[1024,2048]{1,0:T(8,128)(2,1)} %all-gather.3.cloned.1.call-done, bf16[2048,128]{1,0:T(8,128)(2,1)S(1)} %copy-done.6, bf16[2048,128]{1,0:T(8,128)(2,1)} %param.17, bf16[2048,128]{1,0:T(8,128)(2,1)} %param.16), kind=kOutput, calls=%fused_computation.16 | convolution fusion | flops 1615724544 | bytes 6553600 | tf_op jit(solution)/shard_map/dot_general | solution.py:39
  131.9 0.1 multiply_convert_fusion.1
  132.0 3.4 %collective-permute-start = (bf16[2,128]{1,0:T(2,128)(2,1)S(1)}, bf16[2,128]{1,0:T(2,128)(2,1)S(1)}, u32[]{:S(2)}, u32[]{:S(2)}) collective-permute-start(bf16[2,128]{1,0:T(2,128)(2,1)S(1)} %slice.41), channel_id=1, source_target_pairs={{0,8},{8,16},{16,24},{1,9},{9,17},{17,25},{2,10},{10,18},{18,26},{... | collective-permute-start | bytes 1544 | tf_op jit(solution)/shard_map/ppermute | solution.py:12
  135.4 1.3 collective-permute-done
  136.7 3.3 %convolution_convert_fusion.1 = bf16[1024,2048]{1,0:T(8,128)(2,1)} fusion(bf16[128,2048]{1,0:T(8,128)(2,1)S(1)} %copy-done.2, bf16[1024,128]{1,0:T(8,128)(2,1)S(1)} %multiply_convert_fusion.1, bf16[2,128]{1,0:T(2,128)(2,1)S(1)} %collective-permute-done, bf16[1024,384]{1,0:T(8,128)(2,1)S(1)} %fusion.11, f32[128]{0:T(128)S(1)} %get-tuple-element.5, ...), kind=kOutput, calls=%fused_computation.2 | convolution fusion | flops 541196288 | bytes 5244928 | tf_op jit(solution)/shard_map/dot_general | solution.py:62
  140.0 0.0 reduce-scatter.3.cloned.1.call-update
  140.0 0.7 copy-done.3
  140.7 42.5 %reduce-scatter.5.cloned.1.call-done = bf16[144,2048]{1,0:T(8,128)(2,1)} async-done(((bf16[1152,2048]{1,0:T(8,128)(2,1)}), bf16[144,2048]{1,0:T(8,128)(2,1)}) %reduce-scatter.5.cloned.1.call-update) | async-done | bytes 589840 | tf_op jit(solution)/shard_map/reduce_scatter | solution.py:99
  183.2 2.0 reshape.86
  185.2 3.7 %all-to-all-start.1 = ((bf16[4,36,2048]{2,1,0:T(8,128)(2,1)}), bf16[4,36,2048]{2,1,0:T(8,128)(2,1)S(1)}, u32[]{:S(2)}, u32[]{:S(2)}) async-start(bf16[4,36,2048]{2,1,0:T(8,128)(2,1)} %reshape.86), calls=%async_computation.3 | async-start | bytes 1310720 | tf_op jit(solution)/shard_map/all_to_all | solution.py:105
  188.9 0.1 mul.138
  189.0 0.1 copy.22
  189.1 7.4 %all-to-all-done.1 = bf16[4,36,2048]{2,1,0:T(8,128)(2,1)S(1)} async-done(((bf16[4,36,2048]{2,1,0:T(8,128)(2,1)}), bf16[4,36,2048]{2,1,0:T(8,128)(2,1)S(1)}, u32[]{:S(2)}, u32[]{:S(2)}) %all-to-all-start.1) | async-done | bytes 589856 | tf_op jit(solution)/shard_map/all_to_all | solution.py:105
  196.5 0.1 reshape.87
  196.6 1.7 gather_fusion
  198.3 1.7 reshape.88
  200.1 2.2 multiply_reduce_fusion
  202.3 32.0 %reduce-scatter.3.cloned.1.call-done = bf16[128,2048]{1,0:T(8,128)(2,1)} async-done(((bf16[1024,2048]{1,0:T(8,128)(2,1)}), bf16[128,2048]{1,0:T(8,128)(2,1)}) %reduce-scatter.3.cloned.1.call-update) | async-done | bytes 524304 | tf_op jit(solution)/shard_map/reduce_scatter | solution.py:61
  (22 shorter events, 0.1 us)
Async XLA Ops:
  7.2 79.2 %copy-start = (bf16[1,512,2048]{2,1,0:T(8,128)(2,1)S(1)}, bf16[1,512,2048]{2,1,0:T(8,128)(2,1)}, u32[]{:S(2)}) copy-start(bf16[1,512,2048]{2,1,0:T(8,128)(2,1)} %param.27) | copy-start | bytes 6291460
  7.2 72.1 %all-gather.5.cloned.1.call-start = ((), (), s32[]{:S(2)}) async-start(), calls=%async_computation.6 | async-start | bytes 5308416 | tf_op jit(solution)/shard_map/all_gather | solution.py:94
  12.2 16.1 %copy-start.4 = (bf16[2048]{0:T(1024)(128)(2,1)S(1)}, bf16[2048]{0:T(1024)(128)(2,1)}, u32[]{:S(2)}) copy-start(bf16[2048]{0:T(1024)(128)(2,1)} %param.15) | copy-start | bytes 12292
  27.3 2.3 copy-start.1
  28.2 98.9 %all-gather.3.cloned.1.call-start = ((), (), s32[]{:S(2)}) async-start(), calls=%async_computation.4 | async-start | bytes 4718592 | tf_op jit(solution)/shard_map/all_gather | solution.py:40
  30.5 152.6 %reduce-scatter.5.cloned.1.call-start = ((), (), s32[]{:S(2)}) async-start(), calls=%async_computation.7 | async-start | bytes 5308416 | tf_op jit(solution)/shard_map/reduce_scatter | solution.py:99
  97.9 0.7 copy-start.5
  97.9 29.2 %copy-start.6 = (bf16[2048,128]{1,0:T(8,128)(2,1)S(1)}, bf16[2048,128]{1,0:T(8,128)(2,1)}, u32[]{:S(2)}) copy-start(bf16[2048,128]{1,0:T(8,128)(2,1)} %param.18) | copy-start | bytes 1572868
  98.0 136.4 %reduce-scatter.3.cloned.1.call-start = ((), (), s32[]{:S(2)}) async-start(), calls=%async_computation.5 | async-start | bytes 4718592 | tf_op jit(solution)/shard_map/reduce_scatter | solution.py:61
  98.6 38.1 %copy-start.2 = (bf16[128,2048]{1,0:T(8,128)(2,1)S(1)}, bf16[128,2048]{1,0:T(8,128)(2,1)}, u32[]{:S(2)}) copy-start(bf16[128,2048]{1,0:T(8,128)(2,1)} %param.20) | copy-start | bytes 1572868
  132.0 4.7 %collective-permute-start = (bf16[2,128]{1,0:T(2,128)(2,1)S(1)}, bf16[2,128]{1,0:T(2,128)(2,1)S(1)}, u32[]{:S(2)}, u32[]{:S(2)}) collective-permute-start(bf16[2,128]{1,0:T(2,128)(2,1)S(1)} %slice.41), channel_id=1, source_target_pairs={{0,8},{8,16},{16,24},{1,9},{9,17},{17,25},{2,10},{10,18},{18,26},{... | collective-permute-start | bytes 1544 | tf_op jit(solution)/shard_map/ppermute | solution.py:12
  140.0 0.7 copy-start.3
  185.2 11.3 %all-to-all-start.1 = ((bf16[4,36,2048]{2,1,0:T(8,128)(2,1)}), bf16[4,36,2048]{2,1,0:T(8,128)(2,1)S(1)}, u32[]{:S(2)}, u32[]{:S(2)}) async-start(bf16[4,36,2048]{2,1,0:T(8,128)(2,1)} %reshape.86), calls=%async_computation.3 | async-start | bytes 1310720 | tf_op jit(solution)/shard_map/all_to_all | solution.py:105
Sparse Core Ops, SparseCore 0:
  28.3 50.9 all-gather.4
  81.5 45.6 all-gather.2
  129.4 53.6 reduce-scatter.4
  185.9 48.3 reduce-scatter.2
where the time goes:
time: 241 us
  waiting for transfers between devices  160 us (66%)
  matrix products  28 us (12%)
  blocking collectives  14.9 us (6%)
  between operations  13.9 us (6%)
  local copies, waits for them, and re-layouts  9.37 us (4%)
  starting transfers between devices  7.19 us (3%)
  other arithmetic  6.94 us (3%)
    all_gather x1, waiting for transfers between devices, shards(): portion = lax.all_gather(arrived_rows, 'tp', axis=0, tiled=True)  48.7 us
    reduce_scatter x1, waiting for transfers between devices, shards(): lax.psum_scatter(jnp.dot(row_block, w_down, preferred_element_type=jnp.fl...  42.5 us
    reduce_scatter x1, waiting for transfers between devices, shards(): lax.psum_scatter(jnp.dot(row_block, out_proj, preferred_element_type=jnp....  32 us
    all_gather x1, waiting for transfers between devices, shards(): lax.all_gather(normed, 'tp', axis=0, tiled=True)  28.5 us
    all_to_all x1, blocking collectives, shards(): lax.all_to_all(outgoing.reshape(experts, capacity, width_model), 'ep', sp...  14.9 us
    dot_general x1, matrix products, shards(): jnp.dot(row_block, w_down, preferred_element_type=jnp.float32)  11.6 us
    all_to_all x1, waiting for transfers between devices, shards(): lax.all_to_all(summed.reshape(experts, capacity, width_model), 'ep', spli...  7.39 us
    dot_general x1, matrix products, shards(): gate_value = jnp.dot(portion, w_gate, preferred_element_type=jnp.float32)  7.02 us
  transfers between devices with their start and end apart: 6, of which 6 were waited for; matrix products, arithmetic and copies ran while one was open for 15% of the time, Pallas kernels for 0%

commit v1 on v0

v1 whole, which is shorter than its diff:
```python
import functools
import jax
import jax.numpy as jnp
from jax import lax
from jax.experimental import pallas as pl
from jax.experimental.pallas import tpu as pltpu
from jax.sharding import PartitionSpec as P

norm_eps = 1e-06
CORES = 2
ANY = pl.BlockSpec(memory_space=pl.ANY)
VMEM = pl.BlockSpec(memory_space=pltpu.VMEM)
MESH = pl.DeviceIdType.MESH
DMA = pltpu.SemaphoreType.DMA


def from_behind(value, axis, steps):
    count = lax.axis_size(axis)
    leading, last = (max(0, -steps), min(count, count - steps))
    return lax.ppermute(value, axis, [(source, source + steps) for source in range(leading, last)])


def scaled_norm(row_data, gain_vec):
    values = row_data.astype(jnp.float32)
    inverse = lax.rsqrt(jnp.mean(values * values, axis=1, keepdims=True) + norm_eps)
    return (values * inverse * gain_vec.astype(jnp.float32)).astype(jnp.bfloat16)


class Place:
    def __init__(self, n_z, n_ep):
        self.n_z, self.n_ep = n_z, n_ep
        tp = lax.axis_index("tp")
        self.z, self.core = tp // CORES, lax.rem(tp, CORES)
        self.ep = lax.axis_index("ep")
        self.up = {"tp": lax.rem(tp + CORES, n_z * CORES)}
        self.down = {"tp": lax.rem(tp + (n_z - 1) * CORES, n_z * CORES)}
        self.other = {"tp": self.z * CORES + 1 - self.core}
        self.has_up, self.has_down = self.z < n_z - 1, self.z > 0

    def peer(self, offset):
        return {"ep": lax.rem(self.ep + offset, self.n_ep)}

    def source(self, offset):
        return lax.rem(self.ep + self.n_ep - offset, self.n_ep)


def greet(place, line, sibling, peers):
    barrier = pltpu.get_barrier_semaphore()

    def tell(where):
        pl.semaphore_signal(barrier, inc=1, device_id=where, device_id_type=MESH)

    if line:
        pl.when(place.has_up)(lambda: tell(place.up))
        pl.when(place.has_down)(lambda: tell(place.down))
    if sibling:
        tell(place.other)
    if peers:
        for offset in range(1, place.n_ep):
            tell(place.peer(offset))
    count = int(sibling) + (place.n_ep - 1 if peers else 0)
    if line:
        count = count + place.has_up.astype(jnp.int32) + place.has_down.astype(jnp.int32)
    pl.semaphore_wait(barrier, count)


def remote(source, target, send, receive, where):
    return pltpu.make_async_remote_copy(
        src_ref=source,
        dst_ref=target,
        send_sem=send,
        recv_sem=receive,
        device_id=where,
        device_id_type=MESH,
    )


class LineGather:
    def __init__(self, place, own, slot, parts, send, receive, on_arrival=None):
        self.place, self.own, self.slot, self.parts = place, own, slot, parts
        self.send, self.receive, self.on_arrival = send, receive, on_arrival
        self.pending = []

    def hop(self, way, step, part, source, z):
        where = self.place.up if way == 0 else self.place.down
        return remote(
            source,
            self.slot(z, part),
            self.send.at[way, step, part],
            self.receive.at[way, step, part],
            where,
        )

    def go(self, condition, make):
        pl.when(condition)(lambda: make().start())
        self.pending.append((condition, make))

    def begin(self):
        place = self.place
        for part in range(self.parts):
            for way, has in ((0, place.has_up), (1, place.has_down)):
                self.go(
                    has,
                    functools.partial(self.hop, way, 0, part, self.own(part), place.z),
                )

    def step(self, distance):
        place = self.place
        for part in range(self.parts):
            for way in (0, 1):
                if way == 0:
                    z, here, has = place.z - distance, place.z >= distance, place.has_up
                else:
                    z = place.z + distance
                    here, has = z < place.n_z, place.has_down
                z = lax.rem(z + place.n_z, place.n_z)
                incoming = functools.partial(
                    self.hop, way, distance - 1, part, self.own(part), z
                )
                pl.when(here)(lambda incoming=incoming: incoming().wait_recv())
                if distance < place.n_z - 1:
                    self.go(
                        here & has,
                        functools.partial(self.hop, way, distance, part, self.slot(z, part), z),
                    )
                if self.on_arrival is not None:
                    self.on_arrival(here, way, distance, part, z)

    def finish(self):
        for condition, make in self.pending:
            pl.when(condition)(lambda make=make: make().wait_send())


def token_gather_kernel(n_z, n_ep, rows_ref, meta_ref, rows_out, meta_out, sems, meta_sems, local):
    place = Place(n_z, n_ep)
    rows_here = pltpu.make_async_copy(rows_ref, rows_out.at[place.z], local.at[0])
    meta_here = pltpu.make_async_copy(meta_ref, meta_out.at[place.z], local.at[1])
    rows_here.start()
    meta_here.start()
    greet(place, True, False, False)
    half = rows_ref.shape[0] // 2
    gathers = [
        LineGather(
            place,
            lambda part: rows_ref.at[pl.ds(part * half, half)],
            lambda z, part: rows_out.at[z, pl.ds(part * half, half)],
            2,
            sems.at[0],
            sems.at[1],
        ),
        LineGather(
            place,
            lambda part: meta_ref,
            lambda z, part: meta_out.at[z],
            1,
            meta_sems.at[0],
            meta_sems.at[1],
        ),
    ]
    for gather in gathers:
        gather.begin()
    for distance in range(1, n_z):
        for gather in gathers:
            gather.step(distance)
    for gather in gathers:
        gather.finish()
    rows_here.wait()
    meta_here.wait()


def token_gather(n_z, n_ep, rows, meta):
    return pl.pallas_call(
        functools.partial(token_gather_kernel, n_z, n_ep),
        out_shape=(
            jax.ShapeDtypeStruct((n_z,) + rows.shape, rows.dtype),
            jax.ShapeDtypeStruct((n_z,) + meta.shape, meta.dtype),
        ),
        in_specs=[VMEM, VMEM],
        out_specs=(ANY, ANY),
        scratch_shapes=[DMA((2, 2, n_z, 2)), DMA((2, 2, n_z, 1)), DMA((2,))],
        compiler_params=pltpu.CompilerParams(collective_id=0, has_side_effects=True),
        name="token_gather",
    )(rows, meta)


def spread_kernel(
    n_z, n_ep, mix_ref, moe_ref, mix_out, moe_out, sems, share, cross, cross_share, local
):
    place = Place(n_z, n_ep)
    half = mix_ref.shape[0] // 2
    core = place.core
    sharing = []

    def mix_slot(z, part, which):
        return mix_out.at[z, which, pl.ds(part * half, half)]

    def share_copy(slot_here, slot_sem):
        return remote(
            slot_here, slot_here, share.at[0].at[slot_sem], share.at[1].at[slot_sem], place.other
        )

    here = [
        pltpu.make_async_copy(mix_ref, mix_out.at[place.z, core], local.at[0]),
        pltpu.make_async_copy(moe_ref.at[place.ep], moe_out.at[place.ep, core], local.at[1]),
    ]
    for copy in here:
        copy.start()
    greet(place, True, True, True)

    def on_arrival(condition, way, distance, part, z):
        sem = (way * n_z + distance) * 2 + part

        def make():
            return share_copy(mix_slot(z, part, core), sem)

        pl.when(condition)(lambda: make().start())
        sharing.append((condition, make))

    gather = LineGather(
        place,
        lambda part: mix_ref.at[pl.ds(part * half, half)],
        lambda z, part: mix_slot(z, part, core),
        2,
        sems.at[0],
        sems.at[1],
        on_arrival,
    )
    gather.begin()
    crossings = []
    for offset in range(1, n_ep):
        peer = place.peer(offset)
        copy = remote(
            moe_ref.at[peer["ep"]],
            moe_out.at[place.ep, core],
            cross.at[0, offset],
            cross.at[1, offset],
            peer,
        )
        copy.start()
        crossings.append(copy)
    own_mix = remote(mix_ref, mix_out.at[place.z, core], share.at[0, 0], share.at[1, 0], place.other)
    own_mix.start()
    own_moe = remote(
        moe_ref.at[place.ep],
        moe_out.at[place.ep, core],
        cross_share.at[0, 0],
        cross_share.at[1, 0],
        place.other,
    )
    own_moe.start()
    handed = []

    def hand_over(offset):
        crossings[offset - 1].wait_recv()
        slot = moe_out.at[place.source(offset), core]
        copy = remote(
            slot, slot, cross_share.at[0, offset], cross_share.at[1, offset], place.other
        )
        copy.start()
        handed.append(copy)

    order = list(range(1, n_ep))
    for distance in range(1, n_z):
        gather.step(distance)
        count = -(-len(order) // (n_z - distance))
        for offset in order[:count]:
            hand_over(offset)
        order = order[count:]
    gather.finish()
    for copy in crossings:
        copy.wait_send()
    for condition, make in sharing:
        pl.when(condition)(lambda make=make: make().wait())
    for copy in [own_mix, own_moe] + handed:
        copy.wait()
    for copy in here:
        copy.wait()


def spread(n_z, n_ep, mix_rows, moe_rows):
    return pl.pallas_call(
        functools.partial(spread_kernel, n_z, n_ep),
        out_shape=(
            jax.ShapeDtypeStruct((n_z, CORES) + mix_rows.shape, mix_rows.dtype),
            jax.ShapeDtypeStruct((n_ep, CORES) + moe_rows.shape[1:], moe_rows.dtype),
        ),
        in_specs=[VMEM, VMEM],
        out_specs=(ANY, ANY),
        scratch_shapes=[
            DMA((2, 2, n_z, 2)),
            DMA((2, 4 * n_z)),
            DMA((2, n_ep)),
            DMA((2, n_ep)),
            DMA((2,)),
        ],
        compiler_params=pltpu.CompilerParams(collective_id=1, has_side_effects=True),
        name="spread",
    )(mix_rows, moe_rows)


def add_into(target, terms):
    rows = target.shape[0]
    tall = 16 if rows % 16 == 0 else 8

    @pl.loop(0, rows // tall)
    def _(index):
        span = pl.ds(pl.multiple_of(index * tall, tall), tall)
        total = terms[0][span, :].astype(jnp.float32)
        for term in terms[1:]:
            total = total + term[span, :].astype(jnp.float32)
        target[span, :] = total.astype(target.dtype)


class LineReduce:
    def __init__(self, place, terms, total, landing, send, receive):
        self.place, self.terms, self.total, self.landing = place, terms, total, landing
        self.send, self.receive = send, receive
        self.pending = []

    def hop(self, way, z):
        where = self.place.up if way == 0 else self.place.down
        return remote(
            self.total.at[z],
            self.landing.at[way, z],
            self.send.at[z],
            self.receive.at[way, z],
            where,
        )

    def relay(self, way, z):
        place = self.place
        if way == 0:
            active, fed = place.z < z, place.has_down
        else:
            active, fed = place.z > z, place.has_up

        @pl.when(active & fed)
        def _():
            self.hop(way, z).wait_recv()
            add_into(self.total.at[z], self.terms(z) + [self.landing.at[way, z]])

        @pl.when(active & jnp.logical_not(fed))
        def _():
            add_into(self.total.at[z], self.terms(z))

        pl.when(active)(lambda: self.hop(way, z).start())
        self.pending.append((active, way, z))

    def step(self, number, prepare=None):
        for way, z in ((0, self.place.n_z - 1 - number), (1, number)):
            if prepare is not None:
                prepare(z)
            self.relay(way, z)

    def finish(self, out):
        place = self.place
        for z in range(place.n_z):
            landing = [self.landing.at[0, z], self.landing.at[1, z]]
            low, high = z > 0, z < place.n_z - 1

            @pl.when(place.z == z)
            def _(z=z, landing=landing, low=low, high=high):
                terms = self.terms(z)
                if low:
                    self.hop(0, z).wait_recv()
                    terms = terms + [landing[0]]
                if high:
                    self.hop(1, z).wait_recv()
                    terms = terms + [landing[1]]
                add_into(out, terms)

        for active, way, z in self.pending:
            pl.when(active)(lambda way=way, z=z: self.hop(way, z).wait_send())


def collect_kernel(
    n_z,
    n_ep,
    mix_ref,
    moe_ref,
    mix_out,
    moe_out,
    mix_own,
    mix_sib,
    mix_total,
    landing,
    moe_own,
    moe_sib,
    moe_total,
    line_send,
    line_receive,
    load_mix,
    load_moe,
    swap_mix,
    swap_moe,
    cross,
    local,
):
    place = Place(n_z, n_ep)
    core = place.core
    order = []
    for number in range(n_z):
        for z in (n_z - 1 - number, number):
            if z not in order:
                order.append(z)
    mix_loads, moe_loads = {}, []
    for z in order:
        mix_loads[z] = pltpu.make_async_copy(mix_ref.at[z, core], mix_own.at[z], load_mix.at[z])
        mix_loads[z].start()
    offsets = list(range(1, n_ep)) + [0]
    for offset in offsets:
        block = lax.rem(place.ep + offset, n_ep)
        copy = pltpu.make_async_copy(
            moe_ref.at[block, core], moe_own.at[offset], load_moe.at[offset]
        )
        copy.start()
        moe_loads.append(copy)
    greet(place, True, True, True)
    mix_swaps, moe_swaps = {}, []

    def swap(z):
        mix_swaps[z] = remote(
            mix_ref.at[z, 1 - core],
            mix_sib.at[z],
            swap_mix.at[0, z],
            swap_mix.at[1, z],
            place.other,
        )
        mix_swaps[z].start()

    for z in order[:2]:
        swap(z)
    for offset in offsets:
        block = lax.rem(place.ep + offset, n_ep)
        copy = remote(
            moe_ref.at[block, 1 - core],
            moe_sib.at[offset],
            swap_moe.at[0, offset],
            swap_moe.at[1, offset],
            place.other,
        )
        copy.start()
        moe_swaps.append(copy)
    for z in order[2:]:
        swap(z)

    ready = set()

    def prepare(z):
        if z not in ready:
            ready.add(z)
            mix_loads[z].wait()
            mix_swaps[z].wait_recv()

    chain = LineReduce(
        place,
        lambda z: [mix_own.at[z], mix_sib.at[z]],
        mix_total,
        landing,
        line_send,
        line_receive,
    )
    chain.step(0, prepare)
    crossings = []
    for index, offset in enumerate(offsets):
        moe_loads[index].wait()
        moe_swaps[index].wait_recv()
        add_into(moe_total.at[offset], [moe_own.at[offset], moe_sib.at[offset]])
        if offset:
            copy = remote(
                moe_total.at[offset],
                moe_out.at[place.ep],
                cross.at[0, offset],
                cross.at[1, offset],
                place.peer(offset),
            )
            copy.start()
            crossings.append(copy)
    kept = pltpu.make_async_copy(moe_total.at[0], moe_out.at[place.ep], local.at[0])
    kept.start()
    for number in range(1, n_z - 1):
        chain.step(number, prepare)
    for z in order:
        prepare(z)
    chain.finish(mix_out)
    for z in order:
        mix_swaps[z].wait_send()
    for copy in moe_swaps:
        copy.wait_send()
    for copy in crossings:
        copy.wait()
    kept.wait()


def collect(n_z, n_ep, mix_part, moe_part):
    mix_block, moe_block = mix_part.shape[2:], moe_part.shape[2:]
    bf16 = jnp.bfloat16
    return pl.pallas_call(
        functools.partial(collect_kernel, n_z, n_ep),
        out_shape=(
            jax.ShapeDtypeStruct(mix_block, bf16),
            jax.ShapeDtypeStruct((n_ep,) + moe_block, bf16),
        ),
        in_specs=[ANY, ANY],
        out_specs=(VMEM, ANY),
        scratch_shapes=[
            pltpu.VMEM((n_z,) + mix_block, bf16),
            pltpu.VMEM((n_z,) + mix_block, bf16),
            pltpu.VMEM((n_z,) + mix_block, bf16),
            pltpu.VMEM((2, n_z) + mix_block, bf16),
            pltpu.VMEM((n_ep,) + moe_block, bf16),
            pltpu.VMEM((n_ep,) + moe_block, bf16),
            pltpu.VMEM((n_ep,) + moe_block, bf16),
            DMA((n_z,)),
            DMA((2, n_z)),
            DMA((n_z,)),
            DMA((n_ep,)),
            DMA((2, n_z)),
            DMA((2, n_ep)),
            DMA((2, n_ep)),
            DMA((1,)),
        ],
        compiler_params=pltpu.CompilerParams(collective_id=2, has_side_effects=True),
        name="collect",
    )(mix_part, moe_part)


def token_reduce_kernel(n_z, n_ep, part_ref, out_ref, total, landing, send, receive):
    place = Place(n_z, n_ep)
    greet(place, True, False, False)
    chain = LineReduce(place, lambda z: [part_ref.at[z]], total, landing, send, receive)
    for number in range(n_z - 1):
        chain.step(number)
    chain.finish(out_ref)


def token_reduce(n_z, n_ep, part):
    block = part.shape[1:]
    return pl.pallas_call(
        functools.partial(token_reduce_kernel, n_z, n_ep),
        out_shape=jax.ShapeDtypeStruct(block, part.dtype),
        in_specs=[VMEM],
        out_specs=VMEM,
        scratch_shapes=[
            pltpu.VMEM((n_z,) + block, part.dtype),
            pltpu.VMEM((2, n_z) + block, part.dtype),
            DMA((n_z,)),
            DMA((2, n_z)),
        ],
        compiler_params=pltpu.CompilerParams(collective_id=3, has_side_effects=True),
        name="token_reduce",
    )(part)


def shards(
    mix_tokens,
    mix_gain,
    gate_proj,
    conv_proj,
    value_proj,
    conv_taps,
    out_proj,
    moe_tokens,
    moe_gain,
    expert_ids,
    expert_scores,
    expert_gate,
    expert_up,
    expert_down,
):
    n_ep, n_z = lax.axis_size("ep"), lax.axis_size("tp") // CORES
    width_model = moe_tokens.shape[1]
    moe_normed = scaled_norm(moe_tokens, moe_gain)
    experts = expert_gate.shape[0] * n_ep
    row_count, top_count = expert_ids.shape
    capacity = top_count * row_count // experts + max(1, top_count * row_count // (8 * experts))
    slots = n_z * capacity
    flat_ids = expert_ids.reshape(-1)
    onehot = (flat_ids[:, None] == jnp.arange(experts, dtype=jnp.int32)[None, :]).astype(jnp.int32)
    slot_rank = jnp.sum((jnp.cumsum(onehot, axis=0) - onehot) * onehot, axis=1)
    slot_index = flat_ids * slots + (lax.axis_index("tp") // CORES) * capacity + slot_rank
    route_weight = jax.nn.softmax(expert_scores, axis=1)
    meta = jnp.concatenate(
        [slot_index.reshape(row_count, top_count).T.astype(jnp.float32), route_weight.T], axis=0
    )
    lanes = -(-row_count // 128) * 128
    meta = jnp.pad(meta, ((0, -(-2 * top_count // 8) * 8 - 2 * top_count), (0, lanes - row_count)))
    gathered, meta_all = token_gather(n_z, n_ep, moe_normed, meta)
    targets = [
        meta_all[:, k, :row_count].reshape(-1).astype(jnp.int32) for k in range(top_count)
    ]
    weights = [meta_all[:, top_count + k, :row_count].reshape(-1) for k in range(top_count)]
    numbers = jnp.arange(experts * slots, dtype=jnp.int32)
    chosen = sum((numbers[:, None] == target[None, :]).astype(jnp.bfloat16) for target in targets)
    outgoing = jnp.dot(
        chosen, gathered.reshape(-1, width_model), preferred_element_type=jnp.float32
    ).astype(jnp.bfloat16)
    normed = scaled_norm(mix_tokens, mix_gain)
    mix_rows, moe_rows = spread(
        n_z, n_ep, normed, outgoing.reshape(experts, slots, width_model)
    )

    w_joint = jnp.concatenate([gate_proj, conv_proj, value_proj], axis=1)
    combined = jnp.dot(
        mix_rows.reshape(-1, width_model), w_joint, preferred_element_type=jnp.float32
    ).astype(jnp.bfloat16)
    channels = gate_proj.shape[1]
    out_gate = combined[:, :channels]
    in_gate = combined[:, channels : 2 * channels]
    values = combined[:, 2 * channels :]
    signal = (in_gate.astype(jnp.float32) * values.astype(jnp.float32)).astype(jnp.bfloat16)
    tap_count = conv_taps.shape[0]
    before = from_behind(signal[signal.shape[0] - (tap_count - 1) :], "ep", 1)
    portion = moe_rows.reshape(-1, width_model)
    gate_value = jnp.dot(portion, expert_gate[0], preferred_element_type=jnp.float32)
    up_value = jnp.dot(portion, expert_up[0], preferred_element_type=jnp.float32)
    hidden = (jax.nn.silu(gate_value) * up_value).astype(jnp.bfloat16)
    moe_part = jnp.dot(hidden, expert_down[0], preferred_element_type=jnp.float32).astype(
        jnp.bfloat16
    )
    extended = jnp.concatenate([before, signal], axis=0)
    length = signal.shape[0]
    tap_values = conv_taps.astype(jnp.float32)
    convolved = jnp.zeros((length, channels), jnp.float32)
    for offset in range(tap_count):
        convolved = (
            convolved + extended[offset : offset + length].astype(jnp.float32) * tap_values[offset]
        )
    carried = (out_gate.astype(jnp.float32) * convolved).astype(jnp.bfloat16)
    mix_part = jnp.dot(carried, out_proj, preferred_element_type=jnp.float32).astype(jnp.bfloat16)
    mix_out, returned = collect(
        n_z, n_ep, mix_part.reshape(mix_rows.shape), moe_part.reshape(moe_rows.shape)
    )
    mixing = sum(
        jnp.where(target[:, None] == numbers[None, :], weight[:, None], 0.0)
        for target, weight in zip(targets, weights)
    ).astype(jnp.bfloat16)
    moe_part = jnp.dot(
        mixing, returned.reshape(-1, width_model), preferred_element_type=jnp.float32
    ).astype(jnp.bfloat16)
    moe_out = token_reduce(n_z, n_ep, moe_part.reshape(n_z, row_count, width_model))
    return (mix_out, moe_out)


def solution(mesh):
    in_specs = (
        P(("ep", "tp"), None),
        P(),
        P(None, "tp"),
        P(None, "tp"),
        P(None, "tp"),
        P(None, "tp"),
        P("tp", None),
        P(("ep", "tp"), None),
        P(),
        P(("ep", "tp"), None),
        P(("ep", "tp"), None),
        P("ep", None, "tp"),
        P("ep", None, "tp"),
        P("ep", "tp", None),
    )
    out_specs = (P(("ep", "tp"), None), P(("ep", "tp"), None))
    return jax.shard_map(shards, mesh=mesh, in_specs=in_specs, out_specs=out_specs, check_vma=False)
```

time: 241 us -> 219 us (0.909)
  Pallas kernels: 0 us -> 166 us
  waiting for transfers between devices: 160 us -> 0.01 us
  blocking collectives: 14.9 us -> 0 us
  between operations: 13.9 us -> 0.84 us
  local copies, waits for them, and re-layouts: 9.37 us -> 4.77 us
  other arithmetic: 6.94 us -> 11.4 us
  starting transfers between devices: 7.19 us -> 3.39 us
  matrix products: 28 us -> 31.7 us
    pallas_call x0 -> x4, Pallas kernels: none -> 166 us  [the longest x1 57.3 us: collect(): pl.pallas_call(functools.partial(collect_kernel, n_z, n_ep), out_shape=(j...]
    all_gather x2 -> x0, waiting for transfers between devices: 77.2 us -> none  [the longest x1 48.7 us: shards(): portion = lax.all_gather(arrived_rows, 'tp', axis=0, tiled=True)]
    reduce_scatter x2 -> x0, waiting for transfers between devices: 74.5 us -> none  [the longest x1 42.5 us: shards(): lax.psum_scatter(jnp.dot(row_block, w_down, preferred_element_type=jnp.fl...]
    all_to_all x1 -> x0, blocking collectives: 14.9 us -> none  [shards(): lax.all_to_all(outgoing.reshape(experts, capacity, width_model), 'ep', sp...]
    all_to_all x1 -> x0, waiting for transfers between devices: 7.39 us -> none  [shards(): lax.all_to_all(summed.reshape(experts, capacity, width_model), 'ep', spli...]
    all_to_all x1 -> x0, starting transfers between devices: 3.66 us -> none  [shards(): lax.all_to_all(summed.reshape(experts, capacity, width_model), 'ep', spli...]
    dot_general x5 -> x6, matrix products: 28 us -> 31.7 us  [the longest x1 11 us: shards(): jnp.dot(hidden, expert_down[0], preferred_element_type=jnp.float32)]
    reshape x4 -> x0, local copies, waits for them, and re-layouts: 3.17 us -> none  [the longest x1 2.01 us: shards(): summed.reshape(experts, capacity, width_model)]
  transfers between devices with their start and end apart: 6 -> 1, of which waited for: 6 -> 0; matrix products, arithmetic and copies ran while one was open for 15% -> 7% of each run, Pallas kernels for 0% -> 0%
where the time goes in v1:
time: 219 us; the launch traced here: 218 us
  Pallas kernels  166 us (76%)
  matrix products  31.7 us (14%)
  other arithmetic  11.4 us (5%)
  local copies, waits for them, and re-layouts  4.77 us (2%)
  starting transfers between devices  3.39 us (2%)
    pallas_call x1, Pallas kernels, collect(): pl.pallas_call(functools.partial(collect_kernel, n_z, n_ep), out_shape=(j...  57.3 us
    pallas_call x1, Pallas kernels, token_reduce(): pl.pallas_call(functools.partial(token_reduce_kernel, n_z, n_ep), out_sha...  45.1 us
    pallas_call x1, Pallas kernels, spread(): pl.pallas_call(functools.partial(spread_kernel, n_z, n_ep), out_shape=(ja...  40 us
    pallas_call x1, Pallas kernels, token_gather(): pl.pallas_call(functools.partial(token_gather_kernel, n_z, n_ep), out_sha...  23.9 us
    dot_general x1, matrix products, shards(): jnp.dot(hidden, expert_down[0], preferred_element_type=jnp.float32)  11 us
    dot_general x1, matrix products, shards(): jnp.dot(mix_rows.reshape(-1, width_model), w_joint, preferred_element_typ...  5.09 us
  transfers between devices with their start and end apart: 1, of which 0 were waited for; matrix products, arithmetic and copies ran while one was open for 7% of the time, Pallas kernels for 0%

profile of v1, /device:TPU:0, one launch (start us, length us, event | category | flops | bytes accessed | tf_op | source)
XLA Modules:
  0.0 218.3 jit_solution(11946839144579106675)
XLA Ops:
  0.6 0.0 copy-start
  0.6 0.0 copy-start.1
  0.7 0.9 reduce_max.9
  1.5 0.7 fusion.41
  2.2 0.7 divide_bitcast_fusion
  2.9 1.2 fusion.14
  4.2 1.1 fusion.21
  5.3 0.7 convert_element_type.112
  6.0 0.7 convert_element_type.115
  6.7 0.8 copy.18
  7.4 0.1 eq.33
  7.6 0.1 fusion.40
  7.7 0.2 reduce_window_sum.11
  7.8 0.2 select_reduce_fusion
  8.0 0.1 reduce_sum.41
  8.2 0.1 copy.19
  8.2 0.7 convert_bitcast_fusion
  8.9 0.6 select_maximum_fusion.meta_ref
  9.5 1.8 fusion.23.rows_ref
  11.3 23.9 %token_gather.1 = (bf16[4,64,2048]{2,1,0:T(8,128)(2,1)}, f32[4,8,128]{2,1,0:T(8,128)}) custom-call(bf16[64,2048]{1,0:T(8,128)(2,1)} %fusion.23.rows_ref, f32[8,128]{1,0:T(8,128)} %select_maximum_fusion.meta_ref), custom_call_target="tpu_custom_call" | custom-call | tf_op jit(solution)/shard_map/token_gather/pallas_call | solution.py:172
  35.2 0.8 convert_reduce_fusion.1
  36.0 0.1 convert_element_type.121
  36.1 0.1 convert_element_type.124
  36.2 0.0 copy-done.1
  36.2 1.0 fusion.16.mix_ref
  37.2 3.4 %convolution_convert_fusion.2 = bf16[576,2048]{1,0:T(8,128)(2,1)} fusion(bf16[256,2048]{1,0:T(8,128)(2,1)} %bitcast.39, s32[256]{0:T(256)S(1)} %convert_element_type.124, s32[256]{0:T(256)S(1)} %convert_element_type.121), kind=kOutput, calls=%fused_computation.3 | convolution fusion | flops 606339072 | bytes 3409920 | tf_op jit(solution)/shard_map/dot_general | solution.py:595
  40.6 40.0 %spread.1 = (bf16[4,2,128,2048]{3,2,1,0:T(8,128)(2,1)}, bf16[4,2,144,2048]{3,2,1,0:T(8,128)(2,1)}) custom-call(bf16[128,2048]{1,0:T(8,128)(2,1)} %fusion.16.mix_ref, bf16[4,144,2048]{2,1,0:T(8,128)(2,1)} %bitcast.35), custom_call_target="tpu_custom_call" | custom-call | tf_op jit(solution)/shard_map/spread/pallas_call | solution.py:281
  80.6 0.0 copy-start.3
  80.6 0.0 copy-start.4
  80.6 0.0 copy-start.5
  80.6 5.1 %fusion.11 = bf16[1024,384]{1,0:T(8,128)(2,1)S(1)} fusion(bf16[1024,2048]{1,0:T(8,128)(2,1)} %bitcast.42, bf16[2048,128]{1,0:T(8,128)(2,1)} %param.18, bf16[2048,128]{1,0:T(8,128)(2,1)} %param.17, bf16[2048,128]{1,0:T(8,128)(2,1)} %param.16), kind=kOutput, calls=%fused_computation.16 | convolution fusion | flops 1615724544 | bytes 6553600 | tf_op jit(solution)/shard_map/dot_general | solution.py:604
  85.7 0.1 multiply_convert_fusion.1
  85.8 3.4 %collective-permute-start = (bf16[2,128]{1,0:T(2,128)(2,1)S(1)}, bf16[2,128]{1,0:T(2,128)(2,1)S(1)}, u32[]{:S(2)}, u32[]{:S(2)}) collective-permute-start(bf16[2,128]{1,0:T(2,128)(2,1)S(1)} %slice.55), channel_id=1, source_target_pairs={{0,8},{8,16},{16,24},{1,9},{9,17},{17,25},{2,10},{10,18},{18,26},{... | collective-permute-start | bytes 1544 | tf_op jit(solution)/shard_map/ppermute | solution.py:20
  89.2 0.0 copy-done.3
  89.3 0.0 copy-done.4
  89.3 0.0 copy-done.5
  89.3 4.0 %fusion.3 = f32[1152,512]{1,0:T(8,128)} fusion(bf16[1152,2048]{1,0:T(8,128)(2,1)S(1)} %bitcast.41, bf16[1,2048,512]{2,1,0:T(8,128)(2,1)S(1)} %copy-done.5), kind=kOutput, calls=%fused_computation.8 | convolution fusion | flops 2415919104 | bytes 9175040 | tf_op jit(solution)/shard_map/dot_general | solution.py:615
  93.3 11.0 %convolution_convert_fusion = bf16[1152,2048]{1,0:T(8,128)(2,1)} fusion(bf16[1,512,2048]{2,1,0:T(8,128)(2,1)S(1)} %copy-done, bf16[1152,2048]{1,0:T(8,128)(2,1)} %bitcast.40, f32[1152,512]{1,0:T(8,128)} %fusion.3, bf16[1,2048,512]{2,1,0:T(8,128)(2,1)} %param.26), kind=kOutput, calls=%fused_computation | convolution fusion | flops 4837736448 | bytes 15990784 | tf_op jit(solution)/shard_map/dot_general | solution.py:618
  104.3 0.8 slice_reduce_fusion.1
  105.1 0.1 broadcast_in_dim.22
  105.2 0.1 broadcast_in_dim.40
  105.3 0.0 collective-permute-done
  105.3 4.3 %convolution_convert_fusion.1 = bf16[1024,2048]{1,0:T(8,128)(2,1)} fusion(bf16[128,2048]{1,0:T(8,128)(2,1)} %param.20, bf16[1024,128]{1,0:T(8,128)(2,1)S(1)} %multiply_convert_fusion.1, bf16[2,128]{1,0:T(2,128)(2,1)S(1)} %collective-permute-done, bf16[1024,384]{1,0:T(8,128)(2,1)S(1)} %fusion.11, f32[128]{0:T(128)S(1)} %get-tuple-element.19, ...), kind=kOutput, calls=%fused_computation.1 | convolution fusion | flops 541196288 | bytes 5244928 | tf_op jit(solution)/shard_map/dot_general | solution.py:630
  109.6 57.3 %collect.1 = (bf16[128,2048]{1,0:T(8,128)(2,1)}, bf16[4,144,2048]{2,1,0:T(8,128)(2,1)}) custom-call(bf16[4,2,128,2048]{3,2,1,0:T(8,128)(2,1)} %bitcast.36, bf16[4,2,144,2048]{3,2,1,0:T(8,128)(2,1)} %bitcast.37), custom_call_target="tpu_custom_call" | custom-call | tf_op jit(solution)/shard_map/collect/pallas_call | solution.py:498
  167.0 3.8 %convolution_convert_fusion.3 = bf16[256,2048]{1,0:T(8,128)(2,1)} fusion(bf16[576,2048]{1,0:T(8,128)(2,1)} %bitcast.43, f32[256]{0:T(256)S(1)} %broadcast_in_dim.40, s32[256]{0:T(256)S(1)} %convert_element_type.124, f32[256]{0:T(256)S(1)} %broadcast_in_dim.22, s32[256]{0:T(256)S(1)} %convert_element_type.121), kind=kOutput, calls=%fused_computation.5 | convolution fusion | flops 605388800 | bytes 3411968 | tf_op jit(solution)/shard_map/dot_general | solution.py:638
  170.8 45.1 %token_reduce.1 = bf16[64,2048]{1,0:T(8,128)(2,1)} custom-call(bf16[4,64,2048]{2,1,0:T(8,128)(2,1)} %bitcast.38), custom_call_target="tpu_custom_call" | custom-call | tf_op jit(solution)/shard_map/token_reduce/pallas_call | solution.py:539
  215.9 0.8 copy.22
  216.6 1.7 copy.23
  (8 shorter events, 0.0 us)
Async XLA Ops:
  0.6 92.7 %copy-start = (bf16[1,512,2048]{2,1,0:T(8,128)(2,1)S(1)}, bf16[1,512,2048]{2,1,0:T(8,128)(2,1)}, u32[]{:S(2)}) copy-start(bf16[1,512,2048]{2,1,0:T(8,128)(2,1)} %param.27) | copy-start | bytes 6291460
  0.6 35.6 %copy-start.1 = (bf16[128,2048]{1,0:T(8,128)(2,1)S(1)}, bf16[128,2048]{1,0:T(8,128)(2,1)}, u32[]{:S(2)}) copy-start(bf16[128,2048]{1,0:T(8,128)(2,1)} %param.14) | copy-start | bytes 1572868
  80.6 8.6 %copy-start.3 = (bf16[3,128]{1,0:T(4,128)(2,1)S(1)}, bf16[3,128]{1,0:T(4,128)(2,1)}, u32[]{:S(2)}) copy-start(bf16[3,128]{1,0:T(4,128)(2,1)} %param.19) | copy-start | bytes 2308
  80.6 8.7 %copy-start.4 = (bf16[4,2,144,2048]{3,2,1,0:T(8,128)(2,1)S(1)}, bf16[4,2,144,2048]{3,2,1,0:T(8,128)(2,1)}, u32[]{:S(2)}) copy-start(bf16[4,2,144,2048]{3,2,1,0:T(8,128)(2,1)} %get-tuple-element.11) | copy-start | bytes 14155780
  80.6 8.7 %copy-start.5 = (bf16[1,2048,512]{2,1,0:T(8,128)(2,1)S(1)}, bf16[1,2048,512]{2,1,0:T(8,128)(2,1)}, u32[]{:S(2)}) copy-start(bf16[1,2048,512]{2,1,0:T(8,128)(2,1)} %param.25) | copy-start | bytes 6291460
  85.8 19.5 %collective-permute-start = (bf16[2,128]{1,0:T(2,128)(2,1)S(1)}, bf16[2,128]{1,0:T(2,128)(2,1)S(1)}, u32[]{:S(2)}, u32[]{:S(2)}) collective-permute-start(bf16[2,128]{1,0:T(2,128)(2,1)S(1)} %slice.55), channel_id=1, source_target_pairs={{0,8},{8,16},{16,24},{1,9},{9,17},{17,25},{2,10},{10,18},{18,26},{... | collective-permute-start | bytes 1544 | tf_op jit(solution)/shard_map/ppermute | solution.py:20
  166.9 48.9 %copy-start.2 = (bf16[128,2048]{1,0:T(8,128)(2,1)S(1)}, bf16[128,2048]{1,0:T(8,128)(2,1)}, u32[]{:S(2)}) copy-start(bf16[128,2048]{1,0:T(8,128)(2,1)} %get-tuple-element.23) | copy-start | bytes 1572868

commit v2 on v1

--- a/solution.py
+++ b/solution.py
@@ -312,65 +312,85 @@
 
 
 class LineReduce:
-    def __init__(self, place, terms, total, landing, send, receive):
+    def __init__(self, place, terms, total, landing, send, receive, parts=2):
         self.place, self.terms, self.total, self.landing = place, terms, total, landing
-        self.send, self.receive = send, receive
+        self.send, self.receive, self.parts = send, receive, parts
+        self.half = total.shape[1] // parts
         self.pending = []
 
-    def hop(self, way, z):
+    def span(self, ref, part):
+        return ref.at[pl.ds(part * self.half, self.half)]
+
+    def hop(self, way, z, part):
         where = self.place.up if way == 0 else self.place.down
         return remote(
-            self.total.at[z],
-            self.landing.at[way, z],
-            self.send.at[z],
-            self.receive.at[way, z],
+            self.span(self.total.at[z], part),
+            self.span(self.landing.at[way, z], part),
+            self.send.at[z, part],
+            self.receive.at[way, z, part],
             where,
         )
 
-    def relay(self, way, z):
+    def sums(self, z, part, landed=()):
+        add_into(
+            self.span(self.total.at[z], part),
+            [self.span(term, part) for term in self.terms(z)] + list(landed),
+        )
+
+    def lead(self, number, prepare):
         place = self.place
-        if way == 0:
-            active, fed = place.z < z, place.has_down
-        else:
-            active, fed = place.z > z, place.has_up
-
-        @pl.when(active & fed)
-        def _():
-            self.hop(way, z).wait_recv()
-            add_into(self.total.at[z], self.terms(z) + [self.landing.at[way, z]])
-
-        @pl.when(active & jnp.logical_not(fed))
-        def _():
-            add_into(self.total.at[z], self.terms(z))
-
-        pl.when(active)(lambda: self.hop(way, z).start())
-        self.pending.append((active, way, z))
-
-    def step(self, number, prepare=None):
-        for way, z in ((0, self.place.n_z - 1 - number), (1, number)):
-            if prepare is not None:
-                prepare(z)
-            self.relay(way, z)
+        ends = ((0, place.n_z - 1 - number, place.z == 0), (1, number, place.z == place.n_z - 1))
+        for way, z, end in ends:
+            prepare(z)
+        for way, z, end in ends:
+            for part in range(self.parts):
+
+                @pl.when(end)
+                def _(way=way, z=z, part=part):
+                    self.sums(z, part)
+                    self.hop(way, z, part).start()
+
+                self.pending.append((end, way, z, part))
+
+    def relay(self):
+        place, parts = self.place, self.parts
+        for tick in range(1, (place.n_z - 1) * parts):
+            for way in (0, 1):
+                inner = place.z if way == 0 else place.n_z - 1 - place.z
+                number = tick - inner
+                beyond = (place.n_z - 1 - inner) * parts
+                active = (inner > 0) & (number >= 0) & (number < beyond)
+                safe = lax.rem(number + place.n_z * parts, place.n_z * parts)
+                owner, part = safe // parts, lax.rem(safe, parts)
+                z = place.n_z - 1 - owner if way == 0 else owner
+
+                @pl.when(active)
+                def _(way=way, z=z, part=part):
+                    hop = self.hop(way, z, part)
+                    hop.wait_recv()
+                    self.sums(z, part, [self.span(self.landing.at[way, z], part)])
+                    hop.start()
+
+                self.pending.append((active, way, z, part))
 
     def finish(self, out):
         place = self.place
-        for z in range(place.n_z):
-            landing = [self.landing.at[0, z], self.landing.at[1, z]]
-            low, high = z > 0, z < place.n_z - 1
-
-            @pl.when(place.z == z)
-            def _(z=z, landing=landing, low=low, high=high):
-                terms = self.terms(z)
-                if low:
-                    self.hop(0, z).wait_recv()
-                    terms = terms + [landing[0]]
-                if high:
-                    self.hop(1, z).wait_recv()
-                    terms = terms + [landing[1]]
-                add_into(out, terms)
-
-        for active, way, z in self.pending:
-            pl.when(active)(lambda way=way, z=z: self.hop(way, z).wait_send())
+        for part in range(self.parts):
+            for z in range(place.n_z):
+
+                @pl.when(place.z == z)
+                def _(z=z, part=part):
+                    terms = [self.span(term, part) for term in self.terms(z)]
+                    for way, fed in ((0, z > 0), (1, z < place.n_z - 1)):
+                        if fed:
+                            self.hop(way, z, part).wait_recv()
+                            terms.append(self.span(self.landing.at[way, z], part))
+                    add_into(self.span(out, part), terms)
+
+        for active, way, z, part in self.pending:
+            pl.when(active)(
+                lambda way=way, z=z, part=part: self.hop(way, z, part).wait_send()
+            )
 
 
 def collect_kernel(
@@ -378,8 +398,9 @@
     n_ep,
     mix_ref,
     moe_ref,
+    mixing_ref,
     mix_out,
-    moe_out,
+    tokens_out,
     mix_own,
     mix_sib,
     mix_total,
@@ -387,14 +408,19 @@
     moe_own,
     moe_sib,
     moe_total,
+    arrived,
+    tokens_own,
+    tokens_total,
+    tokens_landing,
     line_send,
     line_receive,
+    tokens_send,
+    tokens_receive,
     load_mix,
     load_moe,
     swap_mix,
     swap_moe,
     cross,
-    local,
 ):
     place = Place(n_z, n_ep)
     core = place.core
@@ -428,9 +454,7 @@
         )
         mix_swaps[z].start()
 
-    for z in order[:2]:
-        swap(z)
-    for offset in offsets:
+    def swap_rows(offset):
         block = lax.rem(place.ep + offset, n_ep)
         copy = remote(
             moe_ref.at[block, 1 - core],
@@ -441,8 +465,14 @@
         )
         copy.start()
         moe_swaps.append(copy)
+
+    for z in order[:2]:
+        swap(z)
+    swap_rows(offsets[0])
     for z in order[2:]:
         swap(z)
+    for offset in offsets[1:]:
+        swap_rows(offset)
 
     ready = set()
 
@@ -460,49 +490,87 @@
         line_send,
         line_receive,
     )
-    chain.step(0, prepare)
+    chain.lead(0, prepare)
     crossings = []
-    for index, offset in enumerate(offsets):
+
+    def cross_over(index):
+        offset = offsets[index]
         moe_loads[index].wait()
         moe_swaps[index].wait_recv()
-        add_into(moe_total.at[offset], [moe_own.at[offset], moe_sib.at[offset]])
+        target = moe_total.at[offset] if offset else arrived.at[place.ep]
+        add_into(target, [moe_own.at[offset], moe_sib.at[offset]])
         if offset:
             copy = remote(
                 moe_total.at[offset],
-                moe_out.at[place.ep],
+                arrived.at[place.ep],
                 cross.at[0, offset],
                 cross.at[1, offset],
                 place.peer(offset),
             )
             copy.start()
             crossings.append(copy)
-    kept = pltpu.make_async_copy(moe_total.at[0], moe_out.at[place.ep], local.at[0])
-    kept.start()
+
+    cross_over(0)
     for number in range(1, n_z - 1):
-        chain.step(number, prepare)
+        chain.lead(number, prepare)
+    for index in range(1, n_ep):
+        cross_over(index)
+    chain.relay()
+    for copy in crossings:
+        copy.wait_recv()
+    combine(n_z, n_ep, mixing_ref, arrived, tokens_own)
+    tokens_chain = LineReduce(
+        place,
+        lambda z: [tokens_own.at[z]],
+        tokens_total,
+        tokens_landing,
+        tokens_send,
+        tokens_receive,
+    )
+    for number in range(n_z - 1):
+        tokens_chain.lead(number, lambda z: None)
     for z in order:
         prepare(z)
     chain.finish(mix_out)
+    tokens_chain.relay()
+    tokens_chain.finish(tokens_out)
     for z in order:
         mix_swaps[z].wait_send()
-    for copy in moe_swaps:
+    for copy in moe_swaps + crossings:
         copy.wait_send()
-    for copy in crossings:
-        copy.wait()
-    kept.wait()
-
-
-def collect(n_z, n_ep, mix_part, moe_part):
+
+
+def combine(n_z, n_ep, mixing_ref, arrived, tokens_own):
+    rows, width = tokens_own.shape[1], tokens_own.shape[2]
+    tile = 256 if width % 256 == 0 else width
+
+    @pl.loop(0, width // tile)
+    def _(index):
+        columns = pl.ds(pl.multiple_of(index * tile, tile), tile)
+        total = jnp.zeros((n_z * rows, tile), jnp.float32)
+        for expert in range(n_ep):
+            total = total + jnp.dot(
+                mixing_ref[expert],
+                arrived[expert, :, columns],
+                preferred_element_type=jnp.float32,
+            )
+        total = total.astype(tokens_own.dtype)
+        for z in range(n_z):
+            tokens_own[z, :, columns] = total[z * rows : (z + 1) * rows]
+
+
+def collect(n_z, n_ep, mix_part, moe_part, mixing):
     mix_block, moe_block = mix_part.shape[2:], moe_part.shape[2:]
+    tokens_block = (mixing.shape[1] // n_z, moe_block[1])
     bf16 = jnp.bfloat16
     return pl.pallas_call(
         functools.partial(collect_kernel, n_z, n_ep),
         out_shape=(
             jax.ShapeDtypeStruct(mix_block, bf16),
-            jax.ShapeDtypeStruct((n_ep,) + moe_block, bf16),
+            jax.ShapeDtypeStruct(tokens_block, bf16),
         ),
-        in_specs=[ANY, ANY],
-        out_specs=(VMEM, ANY),
+        in_specs=[ANY, ANY, VMEM],
+        out_specs=(VMEM, VMEM),
         scratch_shapes=[
             pltpu.VMEM((n_z,) + mix_block, bf16),
             pltpu.VMEM((n_z,) + mix_block, bf16),
@@ -511,45 +579,23 @@
             pltpu.VMEM((n_ep,) + moe_block, bf16),
             pltpu.VMEM((n_ep,) + moe_block, bf16),
             pltpu.VMEM((n_ep,) + moe_block, bf16),
-            DMA((n_z,)),
-            DMA((2, n_z)),
+            pltpu.VMEM((n_ep,) + moe_block, bf16),
+            pltpu.VMEM((n_z,) + tokens_block, bf16),
+            pltpu.VMEM((n_z,) + tokens_block, bf16),
+            pltpu.VMEM((2, n_z) + tokens_block, bf16),
+            DMA((n_z, 2)),
+            DMA((2, n_z, 2)),
+            DMA((n_z, 2)),
+            DMA((2, n_z, 2)),
             DMA((n_z,)),
             DMA((n_ep,)),
             DMA((2, n_z)),
             DMA((2, n_ep)),
             DMA((2, n_ep)),
-            DMA((1,)),
         ],
         compiler_params=pltpu.CompilerParams(collective_id=2, has_side_effects=True),
         name="collect",
-    )(mix_part, moe_part)
-
-
-def token_reduce_kernel(n_z, n_ep, part_ref, out_ref, total, landing, send, receive):
-    place = Place(n_z, n_ep)
-    greet(place, True, False, False)
-    chain = LineReduce(place, lambda z: [part_ref.at[z]], total, landing, send, receive)
-    for number in range(n_z - 1):
-        chain.step(number)
-    chain.finish(out_ref)
-
-
-def token_reduce(n_z, n_ep, part):
-    block = part.shape[1:]
-    return pl.pallas_call(
-        functools.partial(token_reduce_kernel, n_z, n_ep),
-        out_shape=jax.ShapeDtypeStruct(block, part.dtype),
-        in_specs=[VMEM],
-        out_specs=VMEM,
-        scratch_shapes=[
-            pltpu.VMEM((n_z,) + block, part.dtype),
-            pltpu.VMEM((2, n_z) + block, part.dtype),
-            DMA((n_z,)),
-            DMA((2, n_z)),
-        ],
-        compiler_params=pltpu.CompilerParams(collective_id=3, has_side_effects=True),
-        name="token_reduce",
-    )(part)
+    )(mix_part, moe_part, mixing)
 
 
 def shards(
@@ -575,14 +621,20 @@
     row_count, top_count = expert_ids.shape
     capacity = top_count * row_count // experts + max(1, top_count * row_count // (8 * experts))
     slots = n_z * capacity
-    flat_ids = expert_ids.reshape(-1)
-    onehot = (flat_ids[:, None] == jnp.arange(experts, dtype=jnp.int32)[None, :]).astype(jnp.int32)
-    slot_rank = jnp.sum((jnp.cumsum(onehot, axis=0) - onehot) * onehot, axis=1)
-    slot_index = flat_ids * slots + (lax.axis_index("tp") // CORES) * capacity + slot_rank
-    route_weight = jax.nn.softmax(expert_scores, axis=1)
-    meta = jnp.concatenate(
-        [slot_index.reshape(row_count, top_count).T.astype(jnp.float32), route_weight.T], axis=0
-    )
+    ids_across = expert_ids.T
+    earlier = jnp.arange(row_count)[:, None] < jnp.arange(row_count)[None, :]
+    same = sum(
+        (expert_ids[:, k][:, None, None] == ids_across[None]).astype(jnp.float32)
+        for k in range(top_count)
+    )
+    slot_rank = jnp.sum(jnp.where(earlier[:, None, :], same, 0.0), axis=0)
+    chip = lax.axis_index("tp") // CORES
+    slot_index = (ids_across * slots + chip * capacity).astype(jnp.float32) + slot_rank
+    scores = [expert_scores[:, k][None, :] for k in range(top_count)]
+    largest = functools.reduce(jnp.maximum, scores)
+    raised = [jnp.exp(score - largest) for score in scores]
+    total = sum(raised)
+    meta = jnp.concatenate([slot_index] + [value / total for value in raised], axis=0)
     lanes = -(-row_count // 128) * 128
     meta = jnp.pad(meta, ((0, -(-2 * top_count // 8) * 8 - 2 * top_count), (0, lanes - row_count)))
     gathered, meta_all = token_gather(n_z, n_ep, moe_normed, meta)
@@ -614,7 +666,9 @@
     portion = moe_rows.reshape(-1, width_model)
     gate_value = jnp.dot(portion, expert_gate[0], preferred_element_type=jnp.float32)
     up_value = jnp.dot(portion, expert_up[0], preferred_element_type=jnp.float32)
-    hidden = (jax.nn.silu(gate_value) * up_value).astype(jnp.bfloat16)
+    hidden = lax.optimization_barrier(
+        (jax.nn.silu(gate_value) * up_value).astype(jnp.bfloat16)
+    )
     moe_part = jnp.dot(hidden, expert_down[0], preferred_element_type=jnp.float32).astype(
         jnp.bfloat16
     )
@@ -628,17 +682,14 @@
         )
     carried = (out_gate.astype(jnp.float32) * convolved).astype(jnp.bfloat16)
     mix_part = jnp.dot(carried, out_proj, preferred_element_type=jnp.float32).astype(jnp.bfloat16)
-    mix_out, returned = collect(
-        n_z, n_ep, mix_part.reshape(mix_rows.shape), moe_part.reshape(moe_rows.shape)
-    )
+    places = numbers.reshape(n_ep, 1, -1)
     mixing = sum(
-        jnp.where(target[:, None] == numbers[None, :], weight[:, None], 0.0)
+        jnp.where(target[None, :, None] == places, weight[None, :, None], 0.0)
         for target, weight in zip(targets, weights)
     ).astype(jnp.bfloat16)
-    moe_part = jnp.dot(
-        mixing, returned.reshape(-1, width_model), preferred_element_type=jnp.float32
-    ).astype(jnp.bfloat16)
-    moe_out = token_reduce(n_z, n_ep, moe_part.reshape(n_z, row_count, width_model))
+    mix_out, moe_out = collect(
+        n_z, n_ep, mix_part.reshape(mix_rows.shape), moe_part.reshape(moe_rows.shape), mixing
+    )
     return (mix_out, moe_out)
 
 

time: 219 us -> 172 us (0.79)
  Pallas kernels: 166 us -> 123 us
  matrix products: 31.7 us -> 26.5 us
    pallas_call x1 -> x0, Pallas kernels: 45.1 us -> none  [token_reduce(): pl.pallas_call(functools.partial(token_reduce_kernel, n_z, n_ep), out_sha...]
    dot_general x1, matrix products: 11 us -> 4.32 us  [shards(): jnp.dot(hidden, expert_down[0], preferred_element_type=jnp.float32)]
  transfers between devices with their start and end apart: 1 -> 1, of which waited for: 0 -> 0; matrix products, arithmetic and copies ran while one was open for 7% -> 10% of each run, Pallas kernels for 0% -> 0%
where the time goes in v2:
time: 172 us; the launch traced here: 171 us
  Pallas kernels  123 us (72%)
  matrix products  26.5 us (15%)
  other arithmetic  12.5 us (7%)
  local copies, waits for them, and re-layouts  5.5 us (3%)
  starting transfers between devices  3.4 us (2%)
    pallas_call x1, Pallas kernels, collect(): pl.pallas_call(functools.partial(collect_kernel, n_z, n_ep), out_shape=(j...  58.8 us
    pallas_call x1, Pallas kernels, spread(): pl.pallas_call(functools.partial(spread_kernel, n_z, n_ep), out_shape=(ja...  40.1 us
    pallas_call x1, Pallas kernels, token_gather(): pl.pallas_call(functools.partial(token_gather_kernel, n_z, n_ep), out_sha...  23.9 us
    dot_general x1, matrix products, shards(): jnp.dot(portion, expert_up[0], preferred_element_type=jnp.float32)  5.38 us
    dot_general x1, matrix products, shards(): jnp.dot(portion, expert_gate[0], preferred_element_type=jnp.float32)  5.23 us
    dot_general x1, matrix products, shards(): jnp.dot(mix_rows.reshape(-1, width_model), w_joint, preferred_element_typ...  4.79 us
    dot_general x1, matrix products, shards(): jnp.dot(hidden, expert_down[0], preferred_element_type=jnp.float32)  4.32 us
    convert_element_type x2, other arithmetic, scaled_norm(): (values * inverse * gain_vec.astype(jnp.float32)).astype(jnp.bfloat16)  3.8 us
  transfers between devices with their start and end apart: 1, of which 0 were waited for; matrix products, arithmetic and copies ran while one was open for 10% of the time, Pallas kernels for 0%

profile of v2, /device:TPU:0, one launch (start us, length us, event | category | flops | bytes accessed | tf_op | source)
XLA Modules:
  0.0 171.4 jit_solution(14339833586832464130)
XLA Ops:
  0.6 0.0 copy-start
  0.7 1.4 fusion.14
  2.1 1.1 fusion.19
  3.2 0.8 add_divide_fusion.1
  4.0 0.8 slice_bitcast_fusion.4
  4.7 0.7 convert_element_type.109
  5.4 0.7 convert_element_type.112
  6.1 0.8 select_reduce_fusion
  6.9 0.7 convert_add_fusion
  7.6 1.8 %fusion.21.rows_ref = bf16[64,2048]{1,0:T(8,128)(2,1)} fusion(bf16[64,2048]{1,0:T(8,128)(2,1)} %param.21, f32[2048]{0:T(1024)S(1)} %convert_element_type.112, f32[64]{0:T(128)S(1)} %add_rsqrt_fusion), kind=kLoop, calls=%fused_computation.30 | loop fusion | flops 524288 | bytes 532736 | tf_op jit(solution)/shard_map/convert_element_type | solution.py:26
  9.3 0.6 select_maximum_fusion.meta_ref
  9.9 23.9 %token_gather.1 = (bf16[4,64,2048]{2,1,0:T(8,128)(2,1)}, f32[4,8,128]{2,1,0:T(8,128)}) custom-call(bf16[64,2048]{1,0:T(8,128)(2,1)} %fusion.21.rows_ref, f32[8,128]{1,0:T(8,128)} %select_maximum_fusion.meta_ref), custom_call_target="tpu_custom_call" | custom-call | tf_op jit(solution)/shard_map/token_gather/pallas_call | solution.py:172
  33.8 0.8 convert_reduce_fusion.1
  34.7 0.1 convert_element_type.118
  34.7 0.1 convert_element_type.121
  34.8 2.0 %fusion.16.mix_ref = bf16[128,2048]{1,0:T(8,128)(2,1)} fusion(bf16[128,2048]{1,0:T(8,128)(2,1)} %param.14, f32[2048]{0:T(1024)S(1)} %convert_element_type.109, f32[128]{0:T(128)S(1)} %add_rsqrt_fusion.1), kind=kLoop, calls=%fused_computation.20 | loop fusion | flops 1048576 | bytes 1057280 | tf_op jit(solution)/shard_map/convert_element_type | solution.py:26
  36.8 3.5 %convolution_convert_fusion.2 = bf16[576,2048]{1,0:T(8,128)(2,1)} fusion(bf16[256,2048]{1,0:T(8,128)(2,1)} %bitcast.58, s32[256]{0:T(256)S(1)} %convert_element_type.121, s32[256]{0:T(256)S(1)} %convert_element_type.118), kind=kOutput, calls=%fused_computation.3 | convolution fusion | flops 606339072 | bytes 3409920 | tf_op jit(solution)/shard_map/dot_general | solution.py:647
  40.3 0.0 copy-start.4
  40.3 40.1 %spread.1 = (bf16[4,2,128,2048]{3,2,1,0:T(8,128)(2,1)}, bf16[4,2,144,2048]{3,2,1,0:T(8,128)(2,1)}) custom-call(bf16[128,2048]{1,0:T(8,128)(2,1)} %fusion.16.mix_ref, bf16[4,144,2048]{2,1,0:T(8,128)(2,1)} %bitcast.55), custom_call_target="tpu_custom_call" | custom-call | tf_op jit(solution)/shard_map/spread/pallas_call | solution.py:281
  80.4 0.0 copy-done.4
  80.4 0.0 copy-start.2
  80.4 4.8 %fusion.11 = bf16[1024,384]{1,0:T(8,128)(2,1)S(1)} fusion(bf16[1024,2048]{1,0:T(8,128)(2,1)} %bitcast.62, bf16[2048,128]{1,0:T(8,128)(2,1)S(1)} %copy-done.4, bf16[2048,128]{1,0:T(8,128)(2,1)} %param.17, bf16[2048,128]{1,0:T(8,128)(2,1)} %param.16), kind=kOutput, calls=%fused_computation.15 | convolution fusion | flops 1615724544 | bytes 6553600 | tf_op jit(solution)/shard_map/dot_general | solution.py:656
  85.2 0.1 multiply_convert_fusion.1
  85.3 3.4 %collective-permute-start = (bf16[2,128]{1,0:T(2,128)(2,1)S(1)}, bf16[2,128]{1,0:T(2,128)(2,1)S(1)}, u32[]{:S(2)}, u32[]{:S(2)}) collective-permute-start(bf16[2,128]{1,0:T(2,128)(2,1)S(1)} %slice.71), channel_id=1, source_target_pairs={{0,8},{8,16},{16,24},{1,9},{9,17},{17,25},{2,10},{10,18},{18,26},{... | collective-permute-start | bytes 1544 | tf_op jit(solution)/shard_map/ppermute | solution.py:20
  88.7 0.8 slice_reduce_fusion.1
  89.5 0.0 copy-done.2
  89.5 0.1 broadcast_in_dim.51
  89.6 0.1 broadcast_in_dim.54
  89.7 0.0 copy-start.3
  89.7 5.2 %fusion.3 = f32[1152,512]{1,0:T(8,128)S(1)} fusion(bf16[1152,2048]{1,0:T(8,128)(2,1)} %bitcast.60, bf16[1,2048,512]{2,1,0:T(8,128)(2,1)} %param.25), kind=kOutput, calls=%fused_computation.7 | convolution fusion | flops 2415919104 | bytes 9175040 | tf_op jit(solution)/shard_map/dot_general | solution.py:667
  94.9 0.0 copy-done.3
  94.9 5.4 %fusion = bf16[1152,512]{1,0:T(8,128)(2,1)S(1)} fusion(bf16[1152,2048]{1,0:T(8,128)(2,1)} %bitcast.61, f32[1152,512]{1,0:T(8,128)S(1)} %fusion.3, bf16[1,2048,512]{2,1,0:T(8,128)(2,1)S(1)} %copy-done.3), kind=kOutput, calls=%fused_computation.4 | convolution fusion | flops 2419458048 | bytes 10354688 | tf_op jit(solution)/shard_map/dot_general | solution.py:668
  100.3 0.0 copy-done
  100.3 0.0 copy-start.1
  100.4 4.3 %convolution_convert_fusion = bf16[1152,2048]{1,0:T(8,128)(2,1)} fusion(bf16[1152,512]{1,0:T(8,128)(2,1)S(1)} %fusion, bf16[1,512,2048]{2,1,0:T(8,128)(2,1)S(1)} %copy-done), kind=kOutput, calls=%fused_computation | convolution fusion | flops 2418278400 | bytes 7995392 | tf_op jit(solution)/shard_map/dot_general | solution.py:672
  104.7 1.0 add_convert_fusion.mixing_ref
  105.7 0.0 collective-permute-done
  105.7 0.0 copy-done.1
  105.7 3.3 %convolution_convert_fusion.1 = bf16[1024,2048]{1,0:T(8,128)(2,1)} fusion(bf16[128,2048]{1,0:T(8,128)(2,1)S(1)} %copy-done.1, bf16[1024,128]{1,0:T(8,128)(2,1)S(1)} %multiply_convert_fusion.1, bf16[2,128]{1,0:T(2,128)(2,1)S(1)} %collective-permute-done, bf16[1024,384]{1,0:T(8,128)(2,1)S(1)} %fusion.11, f32[128]{0:T(128)S(1)} %get-tuple-element.15, ...), kind=kOutput, calls=%fused_computation.1 | convolution fusion | flops 541196288 | bytes 5244928 | tf_op jit(solution)/shard_map/dot_general | solution.py:684
  109.0 58.8 %collect.1 = (bf16[128,2048]{1,0:T(8,128)(2,1)}, bf16[64,2048]{1,0:T(8,128)(2,1)}) custom-call(bf16[4,2,128,2048]{3,2,1,0:T(8,128)(2,1)} %bitcast.56, bf16[4,2,144,2048]{3,2,1,0:T(8,128)(2,1)} %bitcast.57, bf16[4,256,144]{2,1,0:T(8,128)(2,1)} %add_convert_fusion.mixing_ref), custom_call_target="tpu_custom_call" | custom-call | tf_op jit(solution)/shard_map/collect/pallas_call | solution.py:566
  167.9 1.9 %copy.18 = bf16[128,2048]{1,0:T(8,128)(2,1)} copy(bf16[128,2048]{1,0:T(8,128)(2,1)} %get-tuple-element.23) | data formatting | bytes 1048576
  169.7 1.7 copy.19
  (7 shorter events, 0.0 us)
Async XLA Ops:
  0.6 99.7 %copy-start = (bf16[1,512,2048]{2,1,0:T(8,128)(2,1)S(1)}, bf16[1,512,2048]{2,1,0:T(8,128)(2,1)}, u32[]{:S(2)}) copy-start(bf16[1,512,2048]{2,1,0:T(8,128)(2,1)} %param.27) | copy-start | bytes 6291460
  40.3 40.1 %copy-start.4 = (bf16[2048,128]{1,0:T(8,128)(2,1)S(1)}, bf16[2048,128]{1,0:T(8,128)(2,1)}, u32[]{:S(2)}) copy-start(bf16[2048,128]{1,0:T(8,128)(2,1)} %param.18) | copy-start | bytes 1572868
  80.4 9.1 %copy-start.2 = (bf16[3,128]{1,0:T(4,128)(2,1)S(1)}, bf16[3,128]{1,0:T(4,128)(2,1)}, u32[]{:S(2)}) copy-start(bf16[3,128]{1,0:T(4,128)(2,1)} %param.19) | copy-start | bytes 2308
  85.3 20.4 %collective-permute-start = (bf16[2,128]{1,0:T(2,128)(2,1)S(1)}, bf16[2,128]{1,0:T(2,128)(2,1)S(1)}, u32[]{:S(2)}, u32[]{:S(2)}) collective-permute-start(bf16[2,128]{1,0:T(2,128)(2,1)S(1)} %slice.71), channel_id=1, source_target_pairs={{0,8},{8,16},{16,24},{1,9},{9,17},{17,25},{2,10},{10,18},{18,26},{... | collective-permute-start | bytes 1544 | tf_op jit(solution)/shard_map/ppermute | solution.py:20
  89.7 5.2 %copy-start.3 = (bf16[1,2048,512]{2,1,0:T(8,128)(2,1)S(1)}, bf16[1,2048,512]{2,1,0:T(8,128)(2,1)}, u32[]{:S(2)}) copy-start(bf16[1,2048,512]{2,1,0:T(8,128)(2,1)} %param.26) | copy-start | bytes 6291460
  100.3 5.4 %copy-start.1 = (bf16[128,2048]{1,0:T(8,128)(2,1)S(1)}, bf16[128,2048]{1,0:T(8,128)(2,1)}, u32[]{:S(2)}) copy-start(bf16[128,2048]{1,0:T(8,128)(2,1)} %param.20) | copy-start | bytes 1572868
